TPU v7x, 256 devices: a whole 4x4x8 slice. The times are simulated.
256 devices in a mesh: ep: 128 (over z, y, x), tp: 2 (over core).
Axes of the slice: x: 4, y: 4, z: 8, core: 2. Of those that a mesh axis runs over, the one named last changes fastest.
Arguments:
- resid: bfloat16 [2048, 2048], P('ep'), may hold values from -6 to 6
- proj_x: bfloat16 [2048, 2048], P('ep', 'tp'), may hold values from -6 to 6
- proj_z: bfloat16 [2048, 2048], P('ep', 'tp'), may hold values from -6 to 6
- proj_bc: bfloat16 [2048, 2, 512], P('ep', None, 'tp'), may hold values from -6 to 6
- proj_dt: bfloat16 [2048, 32], P('ep', 'tp'), may hold values from -6 to 6
- tail_x: bfloat16 [2048, 3, 2048], P('ep', None, 'tp'), may hold values from -6 to 6
- tail_bc: bfloat16 [2048, 3, 2, 512], P('ep', None, None, 'tp'), may hold values from -6 to 6
- taps_x: bfloat16 [4, 2048], P(None, 'tp'), may hold values from -3 to 3
- taps_bc: bfloat16 [4, 2, 512], P(None, None, 'tp'), may hold values from -3 to 3
- ssm_state: float32 [2048, 32, 4096], P('ep', 'tp'), may hold values from -1.5 to 1.5
- dt_bias: float32 [32], P('tp'), may hold values from -4 to 0
- decay_log: float32 [32], P('tp'), may hold values from -1 to 2.5
- group_gain: float32 [2048], P('tp'), may hold values from 0.1 to 1.9
- out_proj: bfloat16 [2048, 2048], P('tp', 'ep'), may hold values from -0.125 to 0.125
- ffn_gain: float32 [2048], replicated, may hold values from 0.1 to 1.9
- dense_gate: bfloat16 [2048, 4096], P(None, ('ep', 'tp')), may hold values from -0.125 to 0.125
- dense_up: bfloat16 [2048, 4096], P(None, ('ep', 'tp')), may hold values from -0.125 to 0.125
- dense_down: bfloat16 [4096, 2048], P(('ep', 'tp')), may hold values from -0.09375 to 0.09375
- branch_gate: bfloat16 [2048], replicated, may hold values from -0.125 to 0.125
- group_weights: float32 [2048, 4], replicated, may hold values from 0.2 to 1
- expert_ids: int32 [2048, 6], replicated, may hold values from 0 to 127, all different within a row; in each aligned block of 16 rows (0 to 15, 16 to 31, ...) at most 2 rows name the same one
- expert_weights: float32 [2048, 6], replicated, may hold values from 0.1 to 1
- exp_gate: bfloat16 [128, 2048, 512], P('ep', None, 'tp'), may hold values from -0.125 to 0.125
- exp_up: bfloat16 [128, 2048, 512], P('ep', None, 'tp'), may hold values from -0.125 to 0.125
- exp_down: bfloat16 [128, 512, 2048], P('ep', 'tp'), may hold values from -0.25 to 0.25
Outputs:
- out: bfloat16 [2048, 2048], P(('ep', 'tp'))
- new_state: float32 [2048, 32, 4096], P('ep', 'tp')
Inputs may be any that keep to these rules, and one draw needn't show every extreme that they name: `expert_ids`: each row names 6 different experts. In the rows of one index of ep (aligned blocks of 16 rows) no expert is named more than 2 times, a bound that some block reaches.
All inputs are finite; a program needn't handle non-finite values.
Results may differ from a plain program's by a relative error of at most 0.013.
Values may be sent and summed in bfloat16 or wider, within the bound.
A program may use at most 128 MiB of HBM per device.

v0:
```python
import jax
import jax.numpy as jnp
from jax import lax
from jax.sharding import Mesh
from jax.sharding import PartitionSpec as P

HEAD_P = 64
NSTATE = 64
GROUPS = 4
TOPK = 6
HPG = 4
EP = ("ep_0", "ep_1", "ep_2")
EP_TP = ("ep_0", "ep_1", "ep_2", "tp")
EPSILON = 1e-06


def gathered_by_axis(shard, axes, dim):
    if not axes:
        return shard
    nearer = lax.all_gather(shard, axes[-1], axis=dim, tiled=True)
    return gathered_by_axis(nearer, axes[:-1], dim)


def sent_to_all(shard, axis):
    copies = jnp.broadcast_to(shard, (lax.axis_size(axis), *shard.shape))
    return lax.all_to_all(copies, axis, split_axis=0, concat_axis=0, tiled=True)


def of_everyone(shard, axis):
    everything = sent_to_all(shard, axis)
    return jnp.sum(everything.astype(jnp.float32), axis=0)


def split_up(shard, dim, devices):
    before, after = (shard.shape[:dim], shard.shape[dim + 1 :])
    return jnp.moveaxis(shard.reshape(*before, devices, -1, *after), dim, 0)


def sum_at_owner(shard, axis, dim):
    devices = lax.axis_size(axis)
    pieces = lax.all_to_all(split_up(shard, dim, devices), axis, 0, 0, tiled=True)
    return jnp.sum(pieces.astype(jnp.float32), axis=0)


def summed_rows(shard, axes, dim):
    far, near = axes
    pieces = split_up(shard, dim, lax.axis_size(far))
    nearer = sum_at_owner(pieces, near, dim + 1)
    arrived = lax.all_to_all(
        nearer.astype(jnp.bfloat16), far, split_axis=0, concat_axis=0, tiled=True
    )
    return arrived.astype(jnp.float32).sum(axis=0)


def state_update(
    proj_x,
    proj_z,
    proj_bc,
    proj_dt,
    tail_x,
    tail_bc,
    taps_x,
    taps_bc,
    ssm_state,
    dt_bias,
    decay_log,
    group_gain,
):
    window_x = jnp.concatenate([tail_x, proj_x[:, None]], axis=1).astype(jnp.float32)
    conv_x = jax.nn.silu(jnp.sum(window_x * taps_x.astype(jnp.float32)[None], axis=1))
    window_bc = jnp.concatenate([tail_bc, proj_bc[:, None]], axis=1).astype(jnp.float32)
    conv_bc = jax.nn.silu(jnp.sum(window_bc * taps_bc.astype(jnp.float32)[None], axis=1))
    count = proj_x.shape[0]
    heads = proj_dt.shape[1]
    x_heads = conv_x.reshape(count, heads, HEAD_P)
    grouped_bc = conv_bc.reshape(count, 2, heads // HPG, NSTATE)
    input_heads = jnp.repeat(grouped_bc[:, 0], HPG, axis=1)
    read_heads = jnp.repeat(grouped_bc[:, 1], HPG, axis=1)
    step_size = jax.nn.softplus(proj_dt.astype(jnp.float32) + dt_bias)
    decay = jnp.exp(-step_size * jnp.exp(decay_log))
    state = ssm_state.reshape(count, heads, HEAD_P, NSTATE)
    fresh = (step_size[:, :, None] * x_heads)[:, :, :, None] * input_heads[:, :, None, :]
    new_state = decay[:, :, None, None] * state + fresh
    readout = jnp.sum(new_state * read_heads[:, :, None, :], axis=-1)
    gated = readout.reshape(count, heads * HEAD_P) * jax.nn.silu(proj_z.astype(jnp.float32))
    grouped = gated.reshape(count, heads // HPG, HPG * HEAD_P)
    grouped = grouped * lax.rsqrt(jnp.mean(grouped * grouped, axis=-1, keepdims=True) + EPSILON)
    y_out = (grouped.reshape(count, heads * HEAD_P) * group_gain).astype(jnp.bfloat16)
    return (y_out, new_state.reshape(count, heads, HEAD_P * NSTATE))


def shards(
    resid,
    proj_x,
    proj_z,
    proj_bc,
    proj_dt,
    tail_x,
    tail_bc,
    taps_x,
    taps_bc,
    ssm_state,
    dt_bias,
    decay_log,
    group_gain,
    out_proj,
    ffn_gain,
    dense_gate,
    dense_up,
    dense_down,
    branch_gate,
    group_weights,
    expert_ids,
    expert_weights,
    exp_gate,
    exp_up,
    exp_down,
):
    y_out, new_state = state_update(
        proj_x,
        proj_z,
        proj_bc,
        proj_dt,
        tail_x,
        tail_bc,
        taps_x,
        taps_bc,
        ssm_state,
        dt_bias,
        decay_log,
        group_gain,
    )
    partial_value = jnp.dot(
        y_out, gathered_by_axis(out_proj, EP, 1), preferred_element_type=jnp.float32
    )
    mixed = of_everyone(partial_value.astype(jnp.bfloat16), "tp").astype(jnp.float32)
    resid_new = (resid.astype(jnp.float32) + mixed).astype(jnp.bfloat16)
    widened = resid_new.astype(jnp.float32)
    normed = (
        widened
        * lax.rsqrt(jnp.mean(widened * widened, axis=-1, keepdims=True) + EPSILON)
        * ffn_gain
    ).astype(jnp.bfloat16)
    gathered = lax.all_gather(normed, EP, axis=0, tiled=True)
    score = jnp.dot(gathered, branch_gate, preferred_element_type=jnp.float32)
    dense_pre = jnp.dot(gathered, dense_gate, preferred_element_type=jnp.float32)
    dense_lin = jnp.dot(gathered, dense_up, preferred_element_type=jnp.float32)
    dense_hidden = (jax.nn.sigmoid(score)[:, None] * jax.nn.silu(dense_pre) * dense_lin).astype(
        jnp.bfloat16
    )
    experts = lax.axis_size(EP)
    expert_own = lax.axis_index(EP)
    cores = lax.axis_size("tp")
    core_index = lax.axis_index("tp")
    batch = gathered.shape[0]
    rows_each = batch // experts
    half_rows = rows_each // cores
    pairs = rows_each * TOPK
    capacity = (pairs + experts - 1) // experts + 1
    group_size = experts // GROUPS
    levels = jnp.arange(1, capacity + 1, dtype=jnp.int32)
    pair_row = jnp.arange(pairs, dtype=jnp.int32) // TOPK
    pick = (jnp.arange(GROUPS, dtype=jnp.int32) == expert_own // group_size).astype(jnp.float32)
    coarse = jnp.sum(group_weights * pick[None], axis=1)
    pair_weight = (expert_weights * coarse[:, None]).reshape(experts, pairs)
    hits = (expert_ids.reshape(experts, pairs) == expert_own).astype(jnp.int32)
    ranks = jnp.cumsum(hits, axis=1, dtype=jnp.int32)
    select = hits[:, None, :] * (ranks[:, None, :] == levels[None, :, None]).astype(jnp.int32)
    local_row = jnp.sum(select * pair_row[None, None, :], axis=-1, dtype=jnp.int32)
    filled = jnp.sum(select, axis=-1, dtype=jnp.int32).reshape(-1)
    slot_weight = jnp.sum(select.astype(jnp.float32) * pair_weight[:, None, :], axis=-1).reshape(-1)
    row_index = (local_row + jnp.arange(experts, dtype=jnp.int32)[:, None] * rows_each).reshape(-1)
    slot_rows = jnp.take(gathered, row_index, axis=0)
    slot_pre = jnp.dot(slot_rows, exp_gate[0], preferred_element_type=jnp.float32)
    slot_lin = jnp.dot(slot_rows, exp_up[0], preferred_element_type=jnp.float32)
    slot_hidden = (slot_weight[:, None] * jax.nn.silu(slot_pre) * slot_lin).astype(jnp.bfloat16)
    placing = (jnp.arange(batch, dtype=jnp.int32)[:, None] == row_index[None, :]) & (
        filled[None, :] > 0
    )
    row_hidden = jnp.dot(
        placing.astype(jnp.bfloat16), slot_hidden, preferred_element_type=jnp.float32
    ).astype(jnp.bfloat16)
    joined = jnp.concatenate([dense_hidden, row_hidden], axis=1)
    down_all = jnp.concatenate([dense_down, exp_down[0]], axis=0)
    inner_width = joined.shape[1]
    ordered = (
        joined.reshape(experts, cores, half_rows, inner_width)
        .transpose(1, 0, 2, 3)
        .reshape(batch, inner_width)
    )
    halved = sum_at_owner(
        jnp.dot(ordered, down_all, preferred_element_type=jnp.float32).astype(jnp.bfloat16), "tp", 0
    )
    branch = summed_rows(halved.astype(jnp.bfloat16), ("ep_0", ("ep_1", "ep_2")), 0)
    own_rows = lax.dynamic_slice_in_dim(widened, core_index * half_rows, half_rows, 0)
    out = (own_rows + branch).astype(jnp.bfloat16)
    return (out, new_state)


def solution(mesh):
    finer = Mesh(mesh.devices.reshape(8, 4, 4, mesh.shape["tp"]), ("ep_0", "ep_1", "ep_2", "tp"))
    in_specs = (
        P(EP, None),
        P(EP, "tp"),
        P(EP, "tp"),
        P(EP, None, "tp"),
        P(EP, "tp"),
        P(EP, None, "tp"),
        P(EP, None, None, "tp"),
        P(None, "tp"),
        P(None, None, "tp"),
        P(EP, "tp", None),
        P("tp"),
        P("tp"),
        P("tp"),
        P("tp", EP),
        P(),
        P(None, EP_TP),
        P(None, EP_TP),
        P(EP_TP, None),
        P(),
        P(),
        P(),
        P(),
        P(EP, None, "tp"),
        P(EP, None, "tp"),
        P(EP, "tp", None),
    )
    out_specs = (P(EP_TP, None), P(EP, "tp", None))
    return jax.shard_map(
        shards, mesh=finer, in_specs=in_specs, out_specs=out_specs, check_vma=False
    )
```

profile of v0, /device:TPU:8, one launch (start us, length us, event | category | flops | bytes accessed | tf_op | source)
XLA Modules:
  0.0 377.9 jit_solution(146625243671493132)
XLA Ops:
  7.2 12.7 %all_gather.12 = bf16[1024,64]{0,1:T(8,128)(2,1)S(1)} all-gather(bf16[1024,16]{0,1:T(8,128)(2,1)} %param.38), channel_id=1, replica_groups=mesh['ep_0'=8,'ep_1'=4,'ep_2'=4,'tp'=2] {'ep_2'}, dimensions={1}, use_global_device_ids=true | all-gather | bytes 163840 | tf_op jit(solution)/shard_map/all_gather | solution.py:20
  19.9 13.7 %all_gather.13 = bf16[1024,256]{0,1:T(8,128)(2,1)} all-gather(bf16[1024,64]{0,1:T(8,128)(2,1)S(1)} %all_gather.12), channel_id=1, replica_groups=mesh['ep_0'=8,'ep_1'=4,'ep_2'=4,'tp'=2] {'ep_1'}, dimensions={1}, use_global_device_ids=true | all-gather | bytes 655360 | tf_op jit(solution)/shard_map/all_gather | solution.py:20
  33.7 0.7 exp.39
  34.4 0.7 convert_element_type.92
  35.1 0.7 convert_element_type.90
  35.8 0.9 multiply_reduce_fusion.3
  36.7 0.1 reduce_sum.130
  36.8 0.9 multiply_reduce_fusion.1
  37.9 7.9 %reshape.179 = f32[16,16,64,64]{3,2,1,0:T(8,128)} reshape(f32[16,16,4096]{2,1,0:T(8,128)} %param.34) | data formatting | bytes 8388608 | tf_op jit(solution)/shard_map/reshape | solution.py:81
  46.1 8.6 %broadcast_multiply_fusion = (f32[16,16,64,64]{3,2,1,0:T(8,128)}, f32[16,16,64]{2,1,0:T(8,128)S(1)}) fusion(f32[16,16,64]{2,1,0:T(8,128)S(1)} %bitcast.42, f32[16,16,64]{2,1,0:T(8,128)S(1)} %multiply_multiply_fusion, f32[16,16,64]{2,1,0:T(8,128)S(1)} %bitcast.43, f32[16,16,64,64]{3,2,1,0:T(8,128)} %reshape.179, f32[16,16]{1,0:T(8,128)S(1)} %get-tuple-element.11), kind=kLoop, calls=%fused_computation.4 | loop fusion | flops 5226496 | bytes 8651776 | tf_op jit(solution)/shard_map/mul | solution.py:82
  55.0 35.4 %all-gather.3.cloned.1.call-done = bf16[1024,2048]{0,1:T(8,128)(2,1)} async-done(((bf16[1024,256]{0,1:T(8,128)(2,1)}), bf16[1024,2048]{0,1:T(8,128)(2,1)}) %all-gather.3.cloned.1.call-update) | async-done | bytes 4194320 | tf_op jit(solution)/shard_map/all_gather | solution.py:20
  90.5 3.4 convolution_convert_fusion.2
  93.9 3.8 %all_to_all.20 = bf16[2,16,2048]{2,1,0:T(8,128)(2,1)S(1)} all-to-all(bf16[2,16,2048]{2,1,0:T(8,128)(2,1)S(1)} %broadcast_in_dim.21), channel_id=1, replica_groups=mesh['ep_0'=8,'ep_1'=4,'ep_2'=4,'tp'=2] {'tp'}, dimensions={0} | all-to-all | bytes 262144 | tf_op jit(solution)/shard_map/all_to_all | solution.py:26
  97.8 0.1 multiply_reduce_fusion.2
  97.9 0.7 multiply_convert_fusion
  98.7 0.4 copy.48
  99.1 0.5 reshape.184
  99.7 0.1 reduce_window_sum.11
  100.0 0.1 add.161
  100.2 0.1 add.164
  100.4 0.1 copy.52
  100.5 0.1 gt.18
  100.8 0.4 copy.53
  101.2 0.5 mul.286
  101.9 0.1 copy.55
  102.0 0.1 mul.289
  102.2 119.3 %all-gather.5.cloned.1.call-done = bf16[2048,2048]{1,0:T(8,128)(2,1)} async-done(((bf16[16,2048]{1,0:T(8,128)(2,1)}), bf16[2048,2048]{1,0:T(8,128)(2,1)}) %all-gather.5.cloned.1.call-update) | async-done | bytes 8388624 | tf_op jit(solution)/shard_map/all_gather | solution.py:144
  221.5 5.6 %fusion.38 = f32[1,2048]{1,0:T(1,128)S(1)} fusion(bf16[2048,2048]{1,0:T(8,128)(2,1)} %all-gather.5.cloned.1.call-done, bf16[2048,1]{0,1:T(2,128)(2,1)S(1)} %reshape.193), kind=kOutput, calls=%fused_computation.84 | convolution fusion | flops 8388608 | bytes 8400896 | tf_op jit(solution)/shard_map/dot_general | solution.py:145
  227.2 6.8 %gather_fusion = bf16[256,2048]{1,0:T(8,128)(2,1)S(1)} fusion(bf16[2048,2048]{1,0:T(8,128)(2,1)} %all-gather.5.cloned.1.call-done, s32[1024]{0:T(1024)S(1)} %pad_clamp_fusion), kind=kCustom, calls=%fused_computation | custom fusion | bytes 2098176 | tf_op jit(solution)/shard_map/jit(_take)/gather | solution.py:173
  234.0 2.4 fusion.9
  236.5 2.4 convolution_convert_fusion.1
  238.9 5.7 %fusion.39 = f32[2048,16]{0,1:T(8,128)S(1)} fusion(bf16[2048,2048]{1,0:T(8,128)(2,1)} %all-gather.5.cloned.1.call-done, bf16[2048,16]{0,1:T(8,128)(2,1)S(1)} %copy-done.3), kind=kOutput, calls=%fused_computation.85 | convolution fusion | flops 134217728 | bytes 8585216 | tf_op jit(solution)/shard_map/dot_general | solution.py:146
  244.5 5.7 %fusion = bf16[2048,16]{0,1:T(8,128)(2,1)S(1)} fusion(bf16[2048,2048]{1,0:T(8,128)(2,1)} %all-gather.5.cloned.1.call-done, bf16[2048,16]{0,1:T(8,128)(2,1)S(1)} %copy-done.7, f32[2048,16]{0,1:T(8,128)S(1)} %fusion.39, f32[2048]{0:T(1024)S(1)} %add_divide_fusion), kind=kOutput, calls=%fused_computation.8 | convolution fusion | flops 134447104 | bytes 8658944 | tf_op jit(solution)/shard_map/dot_general | solution.py:147
  250.2 1.1 pad_maximum_fusion
  251.3 1.9 copy.57
  253.2 0.2 copy.58
  253.4 4.7 %convolution_convert_fusion = bf16[2048,2048]{1,0:T(8,128)(2,1)S(1)} fusion(bf16[2048,272]{1,0:T(8,128)(2,1)S(1)} %bitcast.41, bf16[256,2048]{1,0:T(8,128)(2,1)S(1)} %bitcast.50, bf16[16,2048]{1,0:T(8,128)(2,1)S(1)} %copy-done.15), kind=kOutput, calls=%fused_computation.2 | convolution fusion | flops 2288123904 | bytes 10616832 | tf_op jit(solution)/shard_map/dot_general | solution.py:192
  258.1 11.7 %all_to_all.21 = bf16[2,1024,2048]{2,1,0:T(8,128)(2,1)} all-to-all(bf16[2,1024,2048]{2,1,0:T(8,128)(2,1)S(1)} %bitcast.39), channel_id=1, replica_groups=mesh['ep_0'=8,'ep_1'=4,'ep_2'=4,'tp'=2] {'tp'}, dimensions={0} | all-to-all | bytes 16777216 | tf_op jit(solution)/shard_map/all_to_all | solution.py:41
  269.9 8.8 %reduce_sum.139 = bf16[1024,2048]{1,0:T(8,128)(2,1)} reduce(bf16[2,1024,2048]{2,1,0:T(8,128)(2,1)} %all_to_all.21, bf16[]{:T(256)} %constant.95.clone.1), dimensions={0}, to_apply=%region_11.12 | reduce | flops 2097152 | bytes 12582914 | tf_op jit(solution)/shard_map/reduce_sum | solution.py:42
  278.6 4.7 %copy.59 = bf16[16,8,8,2048]{3,2,1,0:T(8,128)(2,1)} copy(bf16[16,8,8,2048]{3,2,0,1:T(8,128)(2,1)} %bitcast.38) | data formatting | bytes 8388608 | tf_op jit(solution)/shard_map/transpose | solution.py:36
  283.4 5.7 %all-to-all-start.2 = ((bf16[16,8,8,2048]{3,2,1,0:T(8,128)(2,1)}), bf16[16,8,8,2048]{3,2,1,0:T(8,128)(2,1)}, u32[]{:S(2)}, u32[]{:S(2)}) async-start(bf16[16,8,8,2048]{3,2,1,0:T(8,128)(2,1)} %copy.59), calls=%async_computation.2 | async-start | bytes 8388608 | tf_op jit(solution)/shard_map/all_to_all | solution.py:41
  289.1 7.9 %mul.296 = f32[16,16,4096]{2,1,0:T(8,128)} reshape(f32[16,16,64,64]{3,2,1,0:T(8,128)} %get-tuple-element.6) | data formatting | bytes 8388608 | tf_op jit(solution)/shard_map/mul | solution.py:82
  297.0 54.5 %all-to-all-done.2 = bf16[16,8,8,2048]{3,2,1,0:T(8,128)(2,1)} async-done(((bf16[16,8,8,2048]{3,2,1,0:T(8,128)(2,1)}), bf16[16,8,8,2048]{3,2,1,0:T(8,128)(2,1)}, u32[]{:S(2)}, u32[]{:S(2)}) %all-to-all-start.2) | async-done | bytes 4194336 | tf_op jit(solution)/shard_map/all_to_all | solution.py:41
  351.4 3.7 reduce_sum.140
  355.2 4.1 %all-to-all-start.3 = ((bf16[8,8,2048]{2,1,0:T(8,128)(2,1)}), bf16[8,8,2048]{2,1,0:T(8,128)(2,1)S(1)}, u32[]{:S(2)}, u32[]{:S(2)}) async-start(bf16[8,8,2048]{2,1,0:T(8,128)(2,1)} %reduce_sum.140), calls=%async_computation.3 | async-start | bytes 524288 | tf_op jit(solution)/shard_map/all_to_all | solution.py:49
  359.3 6.6 %multiply_add_fusion = f32[16,16,4096]{2,1,0:T(8,128)} fusion(f32[16,16,4096]{2,1,0:T(8,128)} %mul.296, f32[16,16,4096]{2,1,0:T(8,128)} %param.34, f32[16,16]{1,0:T(8,128)S(1)} %get-tuple-element.11), kind=kLoop, calls=%fused_computation.3 | loop fusion | flops 2097152 | bytes 12583936 | tf_op jit(solution)/shard_map/add | solution.py:83
  365.9 4.4 %all-to-all-done.3 = bf16[8,8,2048]{2,1,0:T(8,128)(2,1)S(1)} async-done(((bf16[8,8,2048]{2,1,0:T(8,128)(2,1)}), bf16[8,8,2048]{2,1,0:T(8,128)(2,1)S(1)}, u32[]{:S(2)}, u32[]{:S(2)}) %all-to-all-start.3) | async-done | bytes 262176 | tf_op jit(solution)/shard_map/all_to_all | solution.py:49
  370.4 0.6 add_convert_fusion.1
  (73 shorter events, 1.6 us)
Async XLA Ops:
  7.2 229.3 %copy-start = (bf16[1,2048,256]{2,1,0:T(8,128)(2,1)S(1)}, bf16[1,2048,256]{2,1,0:T(8,128)(2,1)}, u32[]{:S(2)}) copy-start(bf16[1,2048,256]{2,1,0:T(8,128)(2,1)} %param.48) | copy-start | bytes 3145732
  7.2 83.3 %all-gather.3.cloned.1.call-start = ((), (), s32[]{:S(2)}) async-start(), calls=%async_computation.4 | async-start | bytes 4718592 | tf_op jit(solution)/shard_map/all_gather | solution.py:20
  33.7 187.8 %all-gather.5.cloned.1.call-start = ((), (), s32[]{:S(2)}) async-start(), calls=%async_computation.5 | async-start | bytes 8454144 | tf_op jit(solution)/shard_map/all_gather | solution.py:144
  37.9 7.9 %copy-start.12 = (bf16[16,16]{1,0:T(8,128)(2,1)S(1)}, bf16[16,16]{1,0:T(8,128)(2,1)}, u32[]{:S(2)}) copy-start(bf16[16,16]{1,0:T(8,128)(2,1)} %param.29) | copy-start | bytes 1540
  37.9 7.9 %copy-start.13 = (f32[16]{0:T(128)S(1)}, f32[16]{0:T(128)}, u32[]{:S(2)}) copy-start(f32[16]{0:T(128)} %param.35) | copy-start | bytes 196
  46.0 8.7 %copy-start.2 = (bf16[16,1024]{1,0:T(8,128)(2,1)S(1)}, bf16[16,1024]{1,0:T(8,128)(2,1)}, u32[]{:S(2)}) copy-start(bf16[16,1024]{1,0:T(8,128)(2,1)} %param.27) | copy-start | bytes 98308
  46.0 44.4 %copy-start.10 = (f32[1024]{0:T(1024)S(1)}, f32[1024]{0:T(1024)}, u32[]{:S(2)}) copy-start(f32[1024]{0:T(1024)} %param.37) | copy-start | bytes 12292
  54.6 43.1 %copy-start.4 = (bf16[16,2048]{1,0:T(8,128)(2,1)S(1)}, bf16[16,2048]{1,0:T(8,128)(2,1)}, u32[]{:S(2)}) copy-start(bf16[16,2048]{1,0:T(8,128)(2,1)} %param.25) | copy-start | bytes 196612
  54.6 43.3 %copy-start.9 = (f32[2048]{0:T(1024)S(1)}, f32[2048]{0:T(1024)}, u32[]{:S(2)}) copy-start(f32[2048]{0:T(1024)} %param.39) | copy-start | bytes 24580
  54.6 44.1 %copy-start.5 = (s32[2048,6]{0,1:T(8,128)S(1)}, s32[2048,6]{0,1:T(8,128)}, u32[]{:S(2)}) copy-start(s32[2048,6]{0,1:T(8,128)} %param.45) | copy-start | bytes 147460
  90.4 9.9 %copy-start.11 = (bf16[2048]{0:T(1024)(128)(2,1)S(1)}, bf16[2048]{0:T(1024)(128)(2,1)}, u32[]{:S(2)}) copy-start(bf16[2048]{0:T(1024)(128)(2,1)} %param.43) | copy-start | bytes 12292
  90.4 10.3 %copy-start.8 = (f32[2048,4]{0,1:T(4,128)S(1)}, f32[2048,4]{0,1:T(4,128)}, u32[]{:S(2)}) copy-start(f32[2048,4]{0,1:T(4,128)} %param.44) | copy-start | bytes 98308
  90.4 10.4 %copy-start.6 = (f32[2048,6]{0,1:T(8,128)S(1)}, f32[2048,6]{0,1:T(8,128)}, u32[]{:S(2)}) copy-start(f32[2048,6]{0,1:T(8,128)} %param.46) | copy-start | bytes 147460
  234.0 4.8 %copy-start.3 = (bf16[2048,16]{0,1:T(8,128)(2,1)S(1)}, bf16[2048,16]{0,1:T(8,128)(2,1)}, u32[]{:S(2)}) copy-start(bf16[2048,16]{0,1:T(8,128)(2,1)} %param.40) | copy-start | bytes 196612
  238.8 5.7 %copy-start.7 = (bf16[2048,16]{0,1:T(8,128)(2,1)S(1)}, bf16[2048,16]{0,1:T(8,128)(2,1)}, u32[]{:S(2)}) copy-start(bf16[2048,16]{0,1:T(8,128)(2,1)} %param.41) | copy-start | bytes 196612
  250.2 3.1 copy-start.15
  251.3 2.1 copy-start.14
  283.4 68.1 %all-to-all-start.2 = ((bf16[16,8,8,2048]{3,2,1,0:T(8,128)(2,1)}), bf16[16,8,8,2048]{3,2,1,0:T(8,128)(2,1)}, u32[]{:S(2)}, u32[]{:S(2)}) async-start(bf16[16,8,8,2048]{3,2,1,0:T(8,128)(2,1)} %copy.59), calls=%async_computation.2 | async-start | bytes 8388608 | tf_op jit(solution)/shard_map/all_to_all | solution.py:41
  355.2 15.2 %all-to-all-start.3 = ((bf16[8,8,2048]{2,1,0:T(8,128)(2,1)}), bf16[8,8,2048]{2,1,0:T(8,128)(2,1)S(1)}, u32[]{:S(2)}, u32[]{:S(2)}) async-start(bf16[8,8,2048]{2,1,0:T(8,128)(2,1)} %reduce_sum.140), calls=%async_computation.3 | async-start | bytes 524288 | tf_op jit(solution)/shard_map/all_to_all | solution.py:49
  359.3 11.8 %copy-start.1 = (bf16[1,2048,256]{2,1,0:T(8,128)(2,1)S(1)}, bf16[1,2048,256]{2,1,0:T(8,128)(2,1)}, u32[]{:S(2)}) copy-start(bf16[1,2048,256]{2,1,0:T(8,128)(2,1)} %param.48) | copy-start | bytes 3145732
Sparse Core Ops, SparseCore 0:
  33.8 56.5 all-gather.2
  98.8 122.6 all-gather.4
where the time goes:
time: 379 us; the launch traced here: 378 us
  waiting for transfers between devices  214 us (56%)
  blocking collectives  42 us (11%)
  other arithmetic  34.4 us (9%)
  local copies, waits for them, and re-layouts  33.5 us (9%)
  matrix products  29.9 us (8%)
  between operations  14.5 us (4%)
  starting transfers between devices  9.92 us (3%)
    all_gather x1, waiting for transfers between devices, shards(): gathered = lax.all_gather(normed, EP, axis=0, tiled=True)  119 us
    all_to_all x1, waiting for transfers between devices, sum_at_owner(): lax.all_to_all(split_up(shard, dim, devices), axis, 0, 0, tiled=True)  54.5 us
    all_gather x1, waiting for transfers between devices, gathered_by_axis(): nearer = lax.all_gather(shard, axes[-1], axis=dim, tiled=True)  35.4 us
    all_gather x2, blocking collectives, gathered_by_axis(): nearer = lax.all_gather(shard, axes[-1], axis=dim, tiled=True)  26.4 us
    reduce_sum x2, other arithmetic, sum_at_owner(): return jnp.sum(pieces.astype(jnp.float32), axis=0)  12.5 us
    all_to_all x1, blocking collectives, sum_at_owner(): lax.all_to_all(split_up(shard, dim, devices), axis, 0, 0, tiled=True)  11.7 us
    mul x1, other arithmetic, state_update(): (step_size[:, :, None] * x_heads)[:, :, :, None]  8.56 us
    mul x1, local copies, waits for them, and re-layouts, state_update(): (step_size[:, :, None] * x_heads)[:, :, :, None]  7.88 us
  transfers between devices with their start and end apart: 4, of which 4 were waited for; matrix products, arithmetic and copies ran while one was open for 10% of the time, Pallas kernels for 0%

commit v1 on v0

--- a/solution.py
+++ b/solution.py
@@ -141,7 +141,9 @@
         * lax.rsqrt(jnp.mean(widened * widened, axis=-1, keepdims=True) + EPSILON)
         * ffn_gain
     ).astype(jnp.bfloat16)
-    gathered = lax.all_gather(normed, EP, axis=0, tiled=True)
+    gathered = jnp.concatenate(
+        lax.all_to_all(jnp.stack([normed] * lax.axis_size(EP)), EP, 0, 0), axis=0
+    )
     score = jnp.dot(gathered, branch_gate, preferred_element_type=jnp.float32)
     dense_pre = jnp.dot(gathered, dense_gate, preferred_element_type=jnp.float32)
     dense_lin = jnp.dot(gathered, dense_up, preferred_element_type=jnp.float32)

time: 379 us -> 458 us (1.21)
  waiting for transfers between devices: 214 us -> 279 us
  starting transfers between devices: 9.92 us -> 20.6 us
    all_to_all x0 -> x1, waiting for transfers between devices: none -> 184 us  [shards(): lax.all_to_all(jnp.stack([normed] * lax.axis_size(EP)), EP, 0, 0)]
    all_gather x1 -> x0, waiting for transfers between devices: 119 us -> none  [shards(): gathered = lax.all_gather(normed, EP, axis=0, tiled=True)]
    all_to_all x0 -> x1, starting transfers between devices: none -> 11.7 us  [shards(): lax.all_to_all(jnp.stack([normed] * lax.axis_size(EP)), EP, 0, 0)]
  transfers between devices with their start and end apart: 4 -> 4, of which waited for: 4 -> 4; matrix products, arithmetic and copies ran while one was open for 10% -> 9% of each run, Pallas kernels for 0% -> 0%
where the time goes in v1:
time: 458 us; the launch traced here: 457 us
  waiting for transfers between devices  279 us (61%)
  blocking collectives  42 us (9%)
  local copies, waits for them, and re-layouts  37.7 us (8%)
  other arithmetic  33.8 us (7%)
  matrix products  28.8 us (6%)
  starting transfers between devices  20.6 us (4%)
  between operations  14.5 us (3%)
    all_to_all x1, waiting for transfers between devices, shards(): lax.all_to_all(jnp.stack([normed] * lax.axis_size(EP)), EP, 0, 0)  184 us
    all_to_all x1, waiting for transfers between devices, sum_at_owner(): lax.all_to_all(split_up(shard, dim, devices), axis, 0, 0, tiled=True)  55.2 us
    all_gather x1, waiting for transfers between devices, gathered_by_axis(): nearer = lax.all_gather(shard, axes[-1], axis=dim, tiled=True)  35.5 us
    all_gather x2, blocking collectives, gathered_by_axis(): nearer = lax.all_gather(shard, axes[-1], axis=dim, tiled=True)  26.4 us
    reduce_sum x2, other arithmetic, sum_at_owner(): return jnp.sum(pieces.astype(jnp.float32), axis=0)  12.5 us
    all_to_all x1, blocking collectives, sum_at_owner(): lax.all_to_all(split_up(shard, dim, devices), axis, 0, 0, tiled=True)  11.7 us
    all_to_all x1, starting transfers between devices, shards(): lax.all_to_all(jnp.stack([normed] * lax.axis_size(EP)), EP, 0, 0)  11.7 us
  transfers between devices with their start and end apart: 4, of which 4 were waited for; matrix products, arithmetic and copies ran while one was open for 9% of the time, Pallas kernels for 0%

profile of v1, /device:TPU:8, one launch (start us, length us, event | category | flops | bytes accessed | tf_op | source)
XLA Modules:
  0.0 456.6 jit_solution(13211266088590396823)
XLA Ops:
  7.2 12.7 %all_gather.9 = bf16[1024,64]{0,1:T(8,128)(2,1)S(1)} all-gather(bf16[1024,16]{0,1:T(8,128)(2,1)} %param.38), channel_id=1, replica_groups=mesh['ep_0'=8,'ep_1'=4,'ep_2'=4,'tp'=2] {'ep_2'}, dimensions={1}, use_global_device_ids=true | all-gather | bytes 163840 | tf_op jit(solution)/shard_map/all_gather | solution.py:20
  19.9 13.7 %all_gather.10 = bf16[1024,256]{0,1:T(8,128)(2,1)} all-gather(bf16[1024,64]{0,1:T(8,128)(2,1)S(1)} %all_gather.9), channel_id=1, replica_groups=mesh['ep_0'=8,'ep_1'=4,'ep_2'=4,'tp'=2] {'ep_1'}, dimensions={1}, use_global_device_ids=true | all-gather | bytes 655360 | tf_op jit(solution)/shard_map/all_gather | solution.py:20
  33.7 0.7 exp.39
  34.3 0.7 convert_element_type.92
  35.0 0.7 convert_element_type.90
  35.7 0.9 multiply_reduce_fusion.3
  36.8 0.9 multiply_reduce_fusion.1
  37.8 7.9 %reshape.184 = f32[16,16,64,64]{3,2,1,0:T(8,128)} reshape(f32[16,16,4096]{2,1,0:T(8,128)} %param.34) | data formatting | bytes 8388608 | tf_op jit(solution)/shard_map/reshape | solution.py:81
  46.0 8.6 %broadcast_multiply_fusion = (f32[16,16,64,64]{3,2,1,0:T(8,128)}, f32[16,16,64]{2,1,0:T(8,128)S(1)}) fusion(f32[16,16,64]{2,1,0:T(8,128)S(1)} %bitcast.43, f32[16,16,64]{2,1,0:T(8,128)S(1)} %multiply_multiply_fusion, f32[16,16,64]{2,1,0:T(8,128)S(1)} %bitcast.44, f32[16,16,64,64]{3,2,1,0:T(8,128)} %reshape.184, f32[16,16]{1,0:T(8,128)S(1)} %get-tuple-element.11), kind=kLoop, calls=%fused_computation.4 | loop fusion | flops 5226496 | bytes 8651776 | tf_op jit(solution)/shard_map/mul | solution.py:82
  55.0 35.5 %all-gather.2.cloned.1.call-done = bf16[1024,2048]{0,1:T(8,128)(2,1)} async-done(((bf16[1024,256]{0,1:T(8,128)(2,1)}), bf16[1024,2048]{0,1:T(8,128)(2,1)}) %all-gather.2.cloned.1.call-update) | async-done | bytes 4194320 | tf_op jit(solution)/shard_map/all_gather | solution.py:20
  90.4 3.4 convolution_convert_fusion.2
  93.8 3.8 all_to_all.25
  97.7 0.1 multiply_reduce_fusion.2
  98.0 4.3 stack.2
  102.2 11.7 %all-to-all-start.1 = ((bf16[128,16,2048]{2,1,0:T(8,128)(2,1)}), bf16[128,16,2048]{2,1,0:T(8,128)(2,1)}, u32[]{:S(2)}, u32[]{:S(2)}) async-start(bf16[128,16,2048]{2,1,0:T(8,128)(2,1)} %stack.2), calls=%async_computation.1 | async-start | bytes 16777216 | tf_op jit(solution)/shard_map/all_to_all | solution.py:145
  114.0 0.4 copy.48
  114.3 0.5 reshape.190
  114.9 0.1 reduce_window_sum.11
  115.3 0.1 add.161
  115.5 0.1 add.164
  115.7 0.1 copy.52
  115.8 0.1 gt.18
  116.1 0.4 copy.53
  116.5 0.5 mul.286
  117.2 0.1 copy.55
  117.3 0.1 mul.289
  117.5 183.7 %all-to-all-done.1 = bf16[128,16,2048]{2,1,0:T(8,128)(2,1)} async-done(((bf16[128,16,2048]{2,1,0:T(8,128)(2,1)}), bf16[128,16,2048]{2,1,0:T(8,128)(2,1)}, u32[]{:S(2)}, u32[]{:S(2)}) %all-to-all-start.1) | async-done | bytes 8388640 | tf_op jit(solution)/shard_map/all_to_all | solution.py:145
  301.2 5.7 %fusion.38 = f32[1,2048]{1,0:T(1,128)S(1)} fusion(bf16[2048,2048]{1,0:T(8,128)(2,1)} %bitcast.6, bf16[2048,1]{0,1:T(2,128)(2,1)S(1)} %reshape.199), kind=kOutput, calls=%fused_computation.84 | convolution fusion | flops 8388608 | bytes 8400896 | tf_op jit(solution)/shard_map/dot_general | solution.py:147
  306.9 5.6 %fusion.39 = f32[2048,16]{0,1:T(8,128)S(1)} fusion(bf16[2048,2048]{1,0:T(8,128)(2,1)} %bitcast.6, bf16[2048,16]{0,1:T(8,128)(2,1)S(1)} %copy-done.3), kind=kOutput, calls=%fused_computation.85 | convolution fusion | flops 134217728 | bytes 8585216 | tf_op jit(solution)/shard_map/dot_general | solution.py:148
  312.5 6.9 %gather_fusion = bf16[256,2048]{1,0:T(8,128)(2,1)S(1)} fusion(bf16[2048,2048]{1,0:T(8,128)(2,1)} %bitcast.6, s32[1024]{0:T(1024)S(1)} %pad_clamp_fusion), kind=kCustom, calls=%fused_computation | custom fusion | bytes 2098176 | tf_op jit(solution)/shard_map/jit(_take)/gather | solution.py:175
  319.4 5.7 %fusion = bf16[2048,16]{0,1:T(8,128)(2,1)S(1)} fusion(bf16[2048,2048]{1,0:T(8,128)(2,1)} %bitcast.6, bf16[2048,16]{0,1:T(8,128)(2,1)S(1)} %copy-done.7, f32[2048,16]{0,1:T(8,128)S(1)} %fusion.39, f32[2048]{0:T(1024)S(1)} %add_divide_fusion), kind=kOutput, calls=%fused_computation.8 | convolution fusion | flops 134447104 | bytes 8658944 | tf_op jit(solution)/shard_map/dot_general | solution.py:149
  325.2 1.2 fusion.9
  326.4 2.4 convolution_convert_fusion.1
  328.8 1.1 pad_maximum_fusion
  329.9 1.8 copy.57
  331.7 0.2 copy.58
  331.9 4.7 %convolution_convert_fusion = bf16[2048,2048]{1,0:T(8,128)(2,1)S(1)} fusion(bf16[2048,272]{1,0:T(8,128)(2,1)S(1)} %bitcast.42, bf16[256,2048]{1,0:T(8,128)(2,1)S(1)} %bitcast.51, bf16[16,2048]{1,0:T(8,128)(2,1)S(1)} %copy-done.16), kind=kOutput, calls=%fused_computation.2 | convolution fusion | flops 2288123904 | bytes 10616832 | tf_op jit(solution)/shard_map/dot_general | solution.py:194
  336.6 11.7 %all_to_all.26 = bf16[2,1024,2048]{2,1,0:T(8,128)(2,1)} all-to-all(bf16[2,1024,2048]{2,1,0:T(8,128)(2,1)S(1)} %bitcast.40), channel_id=1, replica_groups=mesh['ep_0'=8,'ep_1'=4,'ep_2'=4,'tp'=2] {'tp'}, dimensions={0} | all-to-all | bytes 16777216 | tf_op jit(solution)/shard_map/all_to_all | solution.py:41
  348.3 8.8 %reduce_sum.139 = bf16[1024,2048]{1,0:T(8,128)(2,1)} reduce(bf16[2,1024,2048]{2,1,0:T(8,128)(2,1)} %all_to_all.26, bf16[]{:T(256)} %constant.95.clone.1), dimensions={0}, to_apply=%region_11.12 | reduce | flops 2097152 | bytes 12582914 | tf_op jit(solution)/shard_map/reduce_sum | solution.py:42
  357.1 4.7 %copy.59 = bf16[16,8,8,2048]{3,2,1,0:T(8,128)(2,1)} copy(bf16[16,8,8,2048]{3,2,0,1:T(8,128)(2,1)} %bitcast.39) | data formatting | bytes 8388608 | tf_op jit(solution)/shard_map/transpose | solution.py:36
  361.9 5.5 %all-to-all-start.3 = ((bf16[16,8,8,2048]{3,2,1,0:T(8,128)(2,1)}), bf16[16,8,8,2048]{3,2,1,0:T(8,128)(2,1)}, u32[]{:S(2)}, u32[]{:S(2)}) async-start(bf16[16,8,8,2048]{3,2,1,0:T(8,128)(2,1)} %copy.59), calls=%async_computation.3 | async-start | bytes 8388608 | tf_op jit(solution)/shard_map/all_to_all | solution.py:41
  367.4 7.9 %mul.296 = f32[16,16,4096]{2,1,0:T(8,128)} reshape(f32[16,16,64,64]{3,2,1,0:T(8,128)} %get-tuple-element.6) | data formatting | bytes 8388608 | tf_op jit(solution)/shard_map/mul | solution.py:82
  375.2 55.2 %all-to-all-done.3 = bf16[16,8,8,2048]{3,2,1,0:T(8,128)(2,1)} async-done(((bf16[16,8,8,2048]{3,2,1,0:T(8,128)(2,1)}), bf16[16,8,8,2048]{3,2,1,0:T(8,128)(2,1)}, u32[]{:S(2)}, u32[]{:S(2)}) %all-to-all-start.3) | async-done | bytes 4194336 | tf_op jit(solution)/shard_map/all_to_all | solution.py:41
  430.5 3.7 reduce_sum.140
  434.2 3.4 all-to-all-start.4
  437.6 6.6 %multiply_add_fusion = f32[16,16,4096]{2,1,0:T(8,128)} fusion(f32[16,16,4096]{2,1,0:T(8,128)} %mul.296, f32[16,16,4096]{2,1,0:T(8,128)} %param.34, f32[16,16]{1,0:T(8,128)S(1)} %get-tuple-element.11), kind=kLoop, calls=%fused_computation.3 | loop fusion | flops 2097152 | bytes 12583936 | tf_op jit(solution)/shard_map/add | solution.py:83
  444.3 4.9 %all-to-all-done.4 = bf16[8,8,2048]{2,1,0:T(8,128)(2,1)S(1)} async-done(((bf16[8,8,2048]{2,1,0:T(8,128)(2,1)}), bf16[8,8,2048]{2,1,0:T(8,128)(2,1)S(1)}, u32[]{:S(2)}, u32[]{:S(2)}) %all-to-all-start.4) | async-done | bytes 262176 | tf_op jit(solution)/shard_map/all_to_all | solution.py:49
  449.2 0.6 add_convert_fusion.1
  (75 shorter events, 1.8 us)
Async XLA Ops:
  7.2 319.2 %copy-start = (bf16[1,2048,256]{2,1,0:T(8,128)(2,1)S(1)}, bf16[1,2048,256]{2,1,0:T(8,128)(2,1)}, u32[]{:S(2)}) copy-start(bf16[1,2048,256]{2,1,0:T(8,128)(2,1)} %param.48) | copy-start | bytes 3145732
  7.2 83.3 %all-gather.2.cloned.1.call-start = ((), (), s32[]{:S(2)}) async-start(), calls=%async_computation.5 | async-start | bytes 4718592 | tf_op jit(solution)/shard_map/all_gather | solution.py:20
  37.8 7.9 %copy-start.12 = (bf16[16,16]{1,0:T(8,128)(2,1)S(1)}, bf16[16,16]{1,0:T(8,128)(2,1)}, u32[]{:S(2)}) copy-start(bf16[16,16]{1,0:T(8,128)(2,1)} %param.29) | copy-start | bytes 1540
  37.8 7.9 %copy-start.13 = (f32[16]{0:T(128)S(1)}, f32[16]{0:T(128)}, u32[]{:S(2)}) copy-start(f32[16]{0:T(128)} %param.35) | copy-start | bytes 196
  46.0 8.7 %copy-start.2 = (bf16[16,1024]{1,0:T(8,128)(2,1)S(1)}, bf16[16,1024]{1,0:T(8,128)(2,1)}, u32[]{:S(2)}) copy-start(bf16[16,1024]{1,0:T(8,128)(2,1)} %param.27) | copy-start | bytes 98308
  46.0 44.4 %copy-start.10 = (f32[1024]{0:T(1024)S(1)}, f32[1024]{0:T(1024)}, u32[]{:S(2)}) copy-start(f32[1024]{0:T(1024)} %param.37) | copy-start | bytes 12292
  54.6 43.1 %copy-start.4 = (bf16[16,2048]{1,0:T(8,128)(2,1)S(1)}, bf16[16,2048]{1,0:T(8,128)(2,1)}, u32[]{:S(2)}) copy-start(bf16[16,2048]{1,0:T(8,128)(2,1)} %param.25) | copy-start | bytes 196612
  54.6 43.3 %copy-start.9 = (f32[2048]{0:T(1024)S(1)}, f32[2048]{0:T(1024)}, u32[]{:S(2)}) copy-start(f32[2048]{0:T(1024)} %param.39) | copy-start | bytes 24580
  102.2 11.7 %copy-start.5 = (s32[2048,6]{0,1:T(8,128)S(1)}, s32[2048,6]{0,1:T(8,128)}, u32[]{:S(2)}) copy-start(s32[2048,6]{0,1:T(8,128)} %param.45) | copy-start | bytes 147460
  102.2 13.4 %copy-start.11 = (bf16[2048]{0:T(1024)(128)(2,1)S(1)}, bf16[2048]{0:T(1024)(128)(2,1)}, u32[]{:S(2)}) copy-start(bf16[2048]{0:T(1024)(128)(2,1)} %param.43) | copy-start | bytes 12292
  102.2 13.7 %copy-start.8 = (f32[2048,4]{0,1:T(4,128)S(1)}, f32[2048,4]{0,1:T(4,128)}, u32[]{:S(2)}) copy-start(f32[2048,4]{0,1:T(4,128)} %param.44) | copy-start | bytes 98308
  102.2 13.8 %copy-start.6 = (f32[2048,6]{0,1:T(8,128)S(1)}, f32[2048,6]{0,1:T(8,128)}, u32[]{:S(2)}) copy-start(f32[2048,6]{0,1:T(8,128)} %param.46) | copy-start | bytes 147460
  102.2 198.9 %all-to-all-start.1 = ((bf16[128,16,2048]{2,1,0:T(8,128)(2,1)}), bf16[128,16,2048]{2,1,0:T(8,128)(2,1)}, u32[]{:S(2)}, u32[]{:S(2)}) async-start(bf16[128,16,2048]{2,1,0:T(8,128)(2,1)} %stack.2), calls=%async_computation.1 | async-start | bytes 16777216 | tf_op jit(solution)/shard_map/all_to_all | solution.py:145
  301.2 5.7 %copy-start.3 = (bf16[2048,16]{0,1:T(8,128)(2,1)S(1)}, bf16[2048,16]{0,1:T(8,128)(2,1)}, u32[]{:S(2)}) copy-start(bf16[2048,16]{0,1:T(8,128)(2,1)} %param.40) | copy-start | bytes 196612
  312.5 6.9 %copy-start.7 = (bf16[2048,16]{0,1:T(8,128)(2,1)S(1)}, bf16[2048,16]{0,1:T(8,128)(2,1)}, u32[]{:S(2)}) copy-start(bf16[2048,16]{0,1:T(8,128)(2,1)} %param.41) | copy-start | bytes 196612
  319.4 5.8 %copy-start.14 = (bf16[1,2048,256]{2,1,0:T(8,128)(2,1)S(1)}, bf16[1,2048,256]{2,1,0:T(8,128)(2,1)}, u32[]{:S(2)}) copy-start(bf16[1,2048,256]{2,1,0:T(8,128)(2,1)} %param.47) | copy-start | bytes 3145732
  328.8 3.1 copy-start.15
  328.8 3.1 copy-start.16
  361.9 68.6 %all-to-all-start.3 = ((bf16[16,8,8,2048]{3,2,1,0:T(8,128)(2,1)}), bf16[16,8,8,2048]{3,2,1,0:T(8,128)(2,1)}, u32[]{:S(2)}, u32[]{:S(2)}) async-start(bf16[16,8,8,2048]{3,2,1,0:T(8,128)(2,1)} %copy.59), calls=%async_computation.3 | async-start | bytes 8388608 | tf_op jit(solution)/shard_map/all_to_all | solution.py:41
  434.2 14.9 %all-to-all-start.4 = ((bf16[8,8,2048]{2,1,0:T(8,128)(2,1)}), bf16[8,8,2048]{2,1,0:T(8,128)(2,1)S(1)}, u32[]{:S(2)}, u32[]{:S(2)}) async-start(bf16[8,8,2048]{2,1,0:T(8,128)(2,1)} %reduce_sum.140), calls=%async_computation.4 | async-start | bytes 524288 | tf_op jit(solution)/shard_map/all_to_all | solution.py:49
  437.6 12.2 %copy-start.1 = (bf16[1,2048,256]{2,1,0:T(8,128)(2,1)S(1)}, bf16[1,2048,256]{2,1,0:T(8,128)(2,1)}, u32[]{:S(2)}) copy-start(bf16[1,2048,256]{2,1,0:T(8,128)(2,1)} %param.48) | copy-start | bytes 3145732
Sparse Core Ops, SparseCore 0:
  33.8 56.5 all-gather.1
